TPU v7x, 32 devices: a whole 2x2x4 slice. The times are simulated.
32 devices in a mesh: grp: 2 (over y), sp: 4 (over z), tp: 4 (over x, core).
Axes of the slice: x: 2, y: 2, z: 4, core: 2. Of those that a mesh axis runs over, the one named last changes fastest.
Arguments:
- tokens: bfloat16 [4096, 2048], P(('grp', 'sp'), 'tp'), parts along dimension 0, may hold values from -140 to 140, as said below
- mix_gain: bfloat16 [2, 2048], replicated, may hold values from 0.099609375 to 1.8984375
- gate_weight: bfloat16 [2, 2048, 2048], P(None, 'sp', 'tp'), may hold values from -0.125 to 0.125
- mix_weight: bfloat16 [2, 2048, 2048], P(None, 'sp', 'tp'), may hold values from -0.125 to 0.125
- value_weight: bfloat16 [2, 2048, 2048], P(None, 'sp', 'tp'), may hold values from -0.125 to 0.125
- out_weight: bfloat16 [2, 2048, 2048], P(None, 'sp', 'tp'), may hold values from -0.125 to 0.125
- conv_taps: bfloat16 [2, 3, 2048], P(None, None, 'tp'), may hold values from -3.5 to 3.5
Outputs:
- result_stream: bfloat16 [4096, 2048], P(('grp', 'sp'), 'tp'), parts along dimension 0
There are 2 independent parts, one for each index of `grp`. A program takes and returns all parts, laid end to end along the dimension named above; an argument that names none is the same for every part. Nothing has to cross between parts.
Inputs may be any that keep to these rules, and one draw needn't show every extreme that they name: `tokens`: activations with feature scales of several sizes.
All inputs are finite; a program needn't handle non-finite values.
Results may differ from a plain program's by a relative error of at most 0.015.
Values may be sent and summed in bfloat16 or wider, within the bound.
A program may use at most 64 MiB of HBM per device.

v0:
```python
import functools

import jax
import jax.numpy as jnp
from jax import lax
from jax.experimental import pallas as pl
from jax.experimental.pallas import tpu as pltpu
from jax.sharding import PartitionSpec as P

EPS = 1e-06
KINDS = 4
MESH = pl.DeviceIdType.MESH


def kernel(sizes, tokens, gain, gate_w, mix_w, value_w, out_w, taps, result,
           wide, acts, carried, gates, edge_out, edge_in, last, swap_in,
           local_sem, w_send, w_recv, a_send, a_recv, e_send, e_recv, r_send, r_recv):
    groups, n, tps, lows = sizes
    highs = tps // lows
    rows, block_width = tokens.shape
    layers = gate_w.shape[0]
    depth = gate_w.shape[1]
    width = block_width // groups
    all_rows = groups * rows
    reach = edge_in.shape[2]
    chunk = min(rows, 256)
    me, my_grp, my_tp = lax.axis_index("sp"), lax.axis_index("grp"), lax.axis_index("tp")
    my_high, my_low = my_tp // lows, lax.rem(my_tp, lows)

    def tp_at(high, low):
        return lax.rem(high + highs, highs) * lows + low

    x_next, x_prev = {"tp": tp_at(my_high + 1, my_low)}, {"tp": tp_at(my_high - 1 + highs, my_low)}
    across = {"grp": lax.rem(my_grp + 1, groups)}
    sibling = {"tp": my_high * lows + (1 - my_low)}
    right, left = {"sp": me + 1}, {"sp": me - 1}

    barrier = pltpu.get_barrier_semaphore()
    fixed = []
    if highs > 1:
        fixed.append(x_next)
    if highs > 2:
        fixed.append(x_prev)
    if groups > 1:
        fixed.append(across)
    if lows > 1:
        fixed.append(sibling)
    for device in fixed:
        pl.semaphore_signal(barrier, inc=1, device_id=device, device_id_type=MESH)

    @pl.when(me > 0)
    def _():
        pl.semaphore_signal(barrier, inc=1, device_id=left, device_id_type=MESH)

    @pl.when(me < n - 1)
    def _():
        pl.semaphore_signal(barrier, inc=1, device_id=right, device_id_type=MESH)

    weights = (gate_w, mix_w, value_w, out_w)
    own_columns = pl.ds(pl.multiple_of(my_grp * width, width), width)

    def w_rows(origin):
        return pl.ds(pl.multiple_of(origin * depth, depth), depth)

    def token_place(g, t, offset, size):
        return (pl.ds(pl.multiple_of(g * rows + offset, size), size),
                pl.ds(pl.multiple_of(t * block_width, block_width), block_width))

    def column_place(g, t, offset, size):
        return (pl.ds(offset, size), pl.ds(pl.multiple_of(t * block_width + g * width, width), width))

    own = column_place(my_grp, my_tp, 0, all_rows)[1]
    locals_ = [pltpu.make_async_copy(tokens, acts.at[(0,) + token_place(my_grp, my_tp, 0, rows)], local_sem.at[0])]
    for m in range(layers * KINDS):
        locals_.append(pltpu.make_async_copy(
            weights[m % KINDS].at[m // KINDS, :, own_columns], wide.at[m, w_rows(me), :], local_sem.at[m + 1]))
    for copy in locals_:
        copy.start()
    for copy in locals_[:4]:
        copy.wait()

    pl.semaphore_wait(barrier, len(fixed) + jnp.minimum(me, 1) + jnp.minimum(n - 1 - me, 1))

    def w_copy(m, origin, way):
        ref = wide.at[m, w_rows(origin), :]
        return pltpu.make_async_remote_copy(
            src_ref=ref, dst_ref=ref, send_sem=w_send.at[m, way, origin], recv_sem=w_recv.at[m, origin],
            device_id=right if way == 0 else left, device_id_type=MESH)

    def w_own(m):
        @pl.when(me < n - 1)
        def _():
            w_copy(m, me, 0).start()

        @pl.when(me > 0)
        def _():
            w_copy(m, me, 1).start()

    def w_event(m, k):
        @pl.when(me - k >= 0)
        def _():
            w_copy(m, me - k, 0).wait_recv()

            @pl.when(me < n - 1)
            def _():
                w_copy(m, me - k, 0).start()

        @pl.when(me + k < n)
        def _():
            w_copy(m, me + k, 1).wait_recv()

            @pl.when(me > 0)
            def _():
                w_copy(m, me + k, 1).start()

    queue = []
    total = layers * KINDS
    ahead = min(3, total)
    lead = 1 * (n - 1)
    for first in range(0, total, KINDS):
        for part in ((0, 1, 2), (3,)):
            for k in range(1, n):
                for j in part:
                    queue.append((first + j, k))
    state = {"issued": ahead, "done": 0}

    def serve(count):
        while count > 0 and state["done"] < len(queue):
            m, k = queue[state["done"]]
            w_event(m, k)
            state["done"] += 1
            count -= 1
            while state["issued"] < total and queue.index((state["issued"], 1)) <= state["done"] + lead:
                w_own(state["issued"])
                state["issued"] += 1

    def serve_until(m):
        while any(q[0] == m for q in queue[state["done"]:]):
            serve(1)

    sends = []

    def gather(index, sems, place, full):
        half = full // 2
        lane = {"next": 0}

        def copy(origin_grp, origin_tp, offset, size, device, slot):
            ref = acts.at[(index,) + place(origin_grp, origin_tp, offset, size)]
            return pltpu.make_async_remote_copy(
                src_ref=ref, dst_ref=ref, send_sem=a_send.at[sems, slot], recv_sem=a_recv.at[sems, slot],
                device_id=device, device_id_type=MESH)

        def send(g, s, offset, size, device, slot):
            c = copy(lax.rem(my_grp + g, groups), tp_at(my_high - s + highs, my_low), offset, size, device, slot)
            c.start()
            sends.append(c)

        def arrived(g, s, offset, size, slot, low=None):
            low = my_low if low is None else low
            copy(lax.rem(my_grp + g, groups), tp_at(my_high - s + highs, low), offset, size, x_next, slot).wait_recv()

        expected = []

        def to_sibling(g, s, offset, size):
            if lows > 1:
                slot = lane["next"]
                lane["next"] += 1
                send(g, s, offset, size, sibling, slot)
                expected.append((g, s, offset, size, slot))

        x_slot = 5 * highs
        y_slot = x_slot + highs
        top_slot, low_slot = y_slot + 1, y_slot + 1 + highs

        def start():
            if highs > 1:
                send(0, 0, 0, full, x_next, x_slot)
            if groups > 1:
                send(0, 0, 0, full, across, y_slot)
            to_sibling(0, 0, 0, full)

        def turn():
            for s in range(1, highs):
                arrived(0, s, 0, full, x_slot + s - 1)
                if groups > 1:
                    send(0, s, 0, half, across, top_slot + s - 1)
                if s < highs - 1:
                    send(0, s, 0, full, x_next, x_slot + s)
                to_sibling(0, s, 0, full)
            if groups > 1:
                arrived(1, 0, 0, full, y_slot)
                if highs > 1:
                    send(1, 0, half, half, x_next, low_slot)
                to_sibling(1, 0, 0, full)

        def finish():
            if groups > 1:
                for s in range(1, highs):
                    arrived(1, s, half, half, low_slot + s - 1)
                    if s < highs - 1:
                        send(1, s, half, half, x_next, low_slot + s)
                    to_sibling(1, s, half, half)
                    arrived(1, s, 0, half, top_slot + s - 1)
                    to_sibling(1, s, 0, half)
            for g, s, offset, size, slot in expected:
                arrived(g, s, offset, size, slot, 1 - my_low)

        return start, turn, finish

    def part_gather(index, part):
        def place(g, t, offset, size):
            return column_place(g, t, part * rows + offset, size)

        return gather(index, index * groups + part, place, rows)

    parts = range(groups)
    for m in range(ahead):
        w_own(m)
    start, turn, finish = gather(0, 0, token_place, rows)
    start()
    for copy in locals_[4:]:
        copy.wait()
    serve(2)
    turn()
    serve(1)
    finish()
    coming = [None] * groups

    chunks = rows // chunk
    for layer in range(layers):
        now, mixed_at = 2 * layer, 2 * layer + 1
        first = layer * KINDS
        for j in range(3):
            serve_until(first + j)

        def project(g, c):
            picked = pl.ds(pl.multiple_of(g * rows + c * chunk, chunk), chunk)
            x = acts[now, picked, :].astype(jnp.float32)
            factor = lax.rsqrt(jnp.mean(x * x, axis=1, keepdims=True) + EPS)
            normed = (x * factor * gain[layer : layer + 1, :].astype(jnp.float32)).astype(jnp.bfloat16)
            gates[picked, :] = jnp.dot(normed, wide[first], preferred_element_type=jnp.float32).astype(jnp.bfloat16)
            inner = jnp.dot(normed, wide[first + 1], preferred_element_type=jnp.float32).astype(jnp.bfloat16)
            values = jnp.dot(normed, wide[first + 2], preferred_element_type=jnp.float32).astype(jnp.bfloat16)
            carried[g, pl.ds(pl.multiple_of(8 + c * chunk, 8), chunk), :] = (
                inner.astype(jnp.float32) * values.astype(jnp.float32))

        def edge(g):
            return pltpu.make_async_remote_copy(
                src_ref=edge_out.at[layer, g], dst_ref=edge_in.at[layer, g], send_sem=e_send.at[layer, g],
                recv_sem=e_recv.at[layer, g], device_id=right, device_id_type=MESH)

        def convolve(g):
            @pl.when(me == 0)
            def _():
                carried[g, 8 - reach : 8, :] = jnp.zeros((reach, width), jnp.float32)

            @pl.when(me > 0)
            def _():
                edge(g).wait_recv()
                carried[g, 8 - reach : 8, :] = edge_in[layer, g]

            conv = jnp.zeros((rows, width), jnp.float32)
            for tap in range(reach + 1):
                row = taps[layer, tap : tap + 1, own_columns].astype(jnp.float32)
                conv = conv + row * carried[g, 8 - reach + tap : 8 - reach + tap + rows, :]
            acts[mixed_at, g * rows : (g + 1) * rows, own] = (
                gates[g * rows : (g + 1) * rows, :].astype(jnp.float32) * conv).astype(jnp.bfloat16)

        going = [part_gather(mixed_at, g) for g in parts]
        for g in parts:
            if coming[g] is not None:
                coming[g][2]()

            @pl.loop(0, chunks)
            def _(i):
                project(g, i)

            edge_out[layer, g] = carried[g, 8 + rows - reach : 8 + rows, :]

            @pl.when(me < n - 1)
            def _():
                edge(g).start()

            if g > 0:
                convolve(g - 1)
                going[g - 1][0]()
        convolve(groups - 1)
        going[groups - 1][0]()

        if layer == 0:
            own_now = pl.ds(pl.multiple_of(my_tp * block_width + my_grp * width, width), width)
        else:
            own_now = own
        coming = [part_gather(now + 2, g) if layer < layers - 1 else None for g in parts]
        for g in parts:
            serve(2)
            going[g][1]()
        serve(1)
        for g in parts:
            going[g][2]()
            serve_until(first + 3)

            @pl.loop(0, chunks)
            def _(c):
                picked = pl.ds(pl.multiple_of(g * rows + c * chunk, chunk), chunk)
                product = jnp.dot(acts[mixed_at, picked, :], wide[first + 3], preferred_element_type=jnp.float32)
                stream = (acts[now, picked, own_now].astype(jnp.float32) + product).astype(jnp.bfloat16)
                if layer < layers - 1:
                    acts[now + 2, picked, own] = stream
                else:
                    last[picked, :] = stream

            if layer < layers - 1:
                coming[g][0]()
        if layer < layers - 1:
            for g in parts:
                serve(2)
                coming[g][1]()
            serve(1)

    mine = pl.ds(pl.multiple_of(my_grp * rows, rows), rows)
    if groups > 1:
        other = lax.rem(my_grp + 1, groups)
        final = pltpu.make_async_remote_copy(
            src_ref=last.at[pl.ds(pl.multiple_of(other * rows, rows), rows), :], dst_ref=swap_in,
            send_sem=r_send, recv_sem=r_recv, device_id=across, device_id_type=MESH)
        final.start()
        result[:, own_columns] = last[mine, :]
        final.wait()
        result[:, pl.ds(pl.multiple_of(other * width, width), width)] = swap_in[...]
    else:
        result[...] = last[...]

    serve(len(queue))
    for c in sends:
        c.wait_send()
    for layer in range(layers):
        for g in parts:
            @pl.when(me < n - 1)
            def _(layer=layer, g=g):
                pltpu.make_async_remote_copy(
                    src_ref=edge_out.at[layer, g], dst_ref=edge_in.at[layer, g], send_sem=e_send.at[layer, g],
                    recv_sem=e_recv.at[layer, g], device_id=right, device_id_type=MESH).wait_send()
    for m in range(total):
        for k in range(n):
            @pl.when((me - k >= 0) & (me < n - 1))
            def _(m=m, k=k):
                w_copy(m, me - k, 0).wait_send()

            @pl.when((me + k < n) & (me > 0))
            def _(m=m, k=k):
                w_copy(m, me + k, 1).wait_send()


def shards(tokens, mix_gain, gate_weight, mix_weight, value_weight, out_weight, conv_taps):
    groups, n, tps = lax.axis_size("grp"), lax.axis_size("sp"), lax.axis_size("tp")
    assert groups <= 2
    lows = 2 if tps % 2 == 0 else 1
    highs = tps // lows
    rows, block_width = tokens.shape
    layers, depth, _ = gate_weight.shape
    reach = conv_taps.shape[1] - 1
    width = block_width // groups
    all_rows, features = groups * rows, tps * block_width
    slots = 5 * highs + 3 * highs + 1
    total = layers * KINDS
    anywhere = pl.BlockSpec(memory_space=pl.ANY)
    vmem = pl.BlockSpec(memory_space=pltpu.VMEM)
    dma = pltpu.SemaphoreType.DMA
    return pl.pallas_call(
        functools.partial(kernel, (groups, n, tps, lows)),
        out_shape=jax.ShapeDtypeStruct(tokens.shape, tokens.dtype),
        in_specs=[anywhere, vmem, anywhere, anywhere, anywhere, anywhere, vmem],
        out_specs=vmem,
        scratch_shapes=[
            pltpu.VMEM((total, n * depth, width), jnp.bfloat16),
            pltpu.VMEM((2 * layers, all_rows, features), jnp.bfloat16),
            pltpu.VMEM((groups, rows + 8, width), jnp.float32),
            pltpu.VMEM((all_rows, width), jnp.bfloat16),
            pltpu.VMEM((layers, groups, reach, width), jnp.float32),
            pltpu.VMEM((layers, groups, reach, width), jnp.float32),
            pltpu.VMEM((all_rows, width), jnp.bfloat16),
            pltpu.VMEM((rows, width), jnp.bfloat16),
            dma((total + 1,)),
            dma((total, 2, n)),
            dma((total, n)),
            dma((2 * layers * groups, slots)),
            dma((2 * layers * groups, slots)),
            dma((layers, groups)),
            dma((layers, groups)),
            dma,
            dma,
        ],
        compiler_params=pltpu.CompilerParams(
            collective_id=0, has_side_effects=True, vmem_limit_bytes=56 * 1024 * 1024
        ),
        name="mixers",
    )(tokens, mix_gain, gate_weight, mix_weight, value_weight, out_weight, conv_taps)


def solution(mesh):
    return jax.shard_map(
        shards,
        mesh=mesh,
        in_specs=(
            P(("grp", "sp"), "tp"),
            P(),
            P(None, "sp", "tp"),
            P(None, "sp", "tp"),
            P(None, "sp", "tp"),
            P(None, "sp", "tp"),
            P(None, None, "tp"),
        ),
        out_specs=P(("grp", "sp"), "tp"),
        check_vma=False,
    )
```

profile of v0, /device:TPU:0, one launch (start us, length us, event | category | flops | bytes accessed | tf_op | source)
XLA Modules:
  0.0 169.1 jit_solution(1540907082487190280)
XLA Ops:
  0.0 1.3 copy.8.taps
  1.3 166.0 %mixers.1 = bf16[512,512]{1,0:T(8,128)(2,1)} custom-call(bf16[512,512]{1,0:T(8,128)(2,1)} %tokens.1, bf16[2,2048]{1,0:T(2,128)(2,1)} %gain.1, bf16[2,512,512]{2,1,0:T(8,128)(2,1)} %gate_w.1, bf16[2,512,512]{2,1,0:T(8,128)(2,1)} %mix_w.1, bf16[2,512,512]{2,1,0:T(8,128)(2,1)} %value_w.1, bf16[2,512,512]{2,1,0:T(8,128)(2,1)} %out_w.1, bf16[2,3,512]{2,1,0:T(4,128)(2,1)} %copy.8.taps), custom_call_target="tpu_custom_call" | custom-call | tf_op jit(solution)/shard_map/mixers/pallas_call | solution.py:370
  167.3 1.9 %copy.10 = bf16[512,512]{1,0:T(8,128)(2,1)} copy(bf16[512,512]{1,0:T(8,128)(2,1)} %mixers.1) | data formatting | bytes 1048576
where the time goes:
time: 169 us
  Pallas kernels  166 us (98%)
  local copies, waits for them, and re-layouts  3.16 us (2%)
    pallas_call x1, Pallas kernels, shards(): pl.pallas_call(functools.partial(kernel, (groups, n, tps, lows)), out_sha...  166 us

commit v1 on v0

v1 whole, which is shorter than its diff:
```python
import functools

import jax
import jax.numpy as jnp
from jax import lax
from jax.experimental import pallas as pl
from jax.experimental.pallas import tpu as pltpu
from jax.sharding import PartitionSpec as P

EPS = 1e-06
KINDS = 4
HALO = 16
PAD = 16
MESH = pl.DeviceIdType.MESH


def when(condition):
    if condition is True:
        return lambda body: body()
    if condition is False:
        return lambda body: None
    return pl.when(condition)


def kernel(sizes, tokens, gain, gate_w, mix_w, value_w, out_w, taps, result,
           wide, acts, tokens_all, normed, carried, gates, mixed, resid, edge_out, edge_in, last, swap_in,
           local_sem, w_send, w_recv, a_send, a_recv, e_send, e_recv, r_send, r_recv, t_send, t_recv, m_send, m_recv):
    groups, n, tps, lows = sizes
    highs = tps // lows
    rows, block_width = tokens.shape
    layers = gate_w.shape[0]
    depth = gate_w.shape[1]
    width = block_width // groups
    reach = edge_in.shape[2]
    total = layers * KINDS
    chunk = min(rows, 256)
    parts = range(groups)
    me, my_grp, my_tp = lax.axis_index("sp"), lax.axis_index("grp"), lax.axis_index("tp")
    my_high, my_low = my_tp // lows, lax.rem(my_tp, lows)

    def tp_at(high, low):
        return lax.rem(high + highs, highs) * lows + low

    x_next, x_prev = {"tp": tp_at(my_high + 1, my_low)}, {"tp": tp_at(my_high - 1 + highs, my_low)}
    across = {"grp": lax.rem(my_grp + 1, groups)}
    sibling = {"tp": my_high * lows + (1 - my_low)}
    right, left = {"sp": me + 1}, {"sp": me - 1}

    lower = 2 * me < n
    step = jnp.where(lower, 1, -1)
    inner, outer = {"sp": me + step}, {"sp": me - step}
    is_end = (me == 0) | (me == n - 1)
    helper = True if n == 4 else (me == 1) | (me == n - 2)
    outer_max = 1 if n == 4 else jnp.where(lower, me, n - 1 - me)
    inner_max = n - 1 - outer_max

    barrier = pltpu.get_barrier_semaphore()
    fixed = []
    if highs > 1:
        fixed.append(x_next)
    if highs > 2:
        fixed.append(x_prev)
    if groups > 1:
        fixed.append(across)
    if lows > 1:
        fixed.append(sibling)
    for device in fixed:
        pl.semaphore_signal(barrier, inc=1, device_id=device, device_id_type=MESH)

    @pl.when(me > 0)
    def _():
        pl.semaphore_signal(barrier, inc=1, device_id=left, device_id_type=MESH)

    @pl.when(me < n - 1)
    def _():
        pl.semaphore_signal(barrier, inc=1, device_id=right, device_id_type=MESH)

    weights = (gate_w, mix_w, value_w, out_w)
    own_columns = pl.ds(pl.multiple_of(my_grp * width, width), width)

    def w_rows(origin):
        return pl.ds(pl.multiple_of(origin * depth, depth), depth)

    def token_place(g, t, offset, size):
        return (pl.ds(pl.multiple_of(g * rows + offset, 8), size),
                pl.ds(pl.multiple_of(t * block_width, block_width), block_width))

    def columns_of(g, t):
        return pl.ds(pl.multiple_of(t * block_width + g * width, width), width)

    own = columns_of(my_grp, my_tp)
    own_slot = jnp.where(me == 1, 1, 0)
    guest_slot = 1 - own_slot
    my_slot = jnp.where(is_end, jnp.where(me == 0, 0, 1), own_slot)

    locals_ = [pltpu.make_async_copy(
        tokens, tokens_all.at[(my_slot,) + token_place(my_grp, my_tp, 0, rows)], local_sem.at[0])]
    for m in range(total):
        locals_.append(pltpu.make_async_copy(
            weights[m % KINDS].at[m // KINDS, :, own_columns], wide.at[m, w_rows(me), :], local_sem.at[m + 1]))
    for copy in locals_:
        copy.start()
    for copy in locals_[:4]:
        copy.wait()

    pl.semaphore_wait(barrier, len(fixed) + jnp.minimum(me, 1) + jnp.minimum(n - 1 - me, 1))

    def w_copy(m, origin, way):
        ref = wide.at[m, w_rows(origin), :]
        return pltpu.make_async_remote_copy(
            src_ref=ref, dst_ref=ref, send_sem=w_send.at[m, way, origin], recv_sem=w_recv.at[m, origin],
            device_id=inner if way == 0 else outer, device_id_type=MESH)

    def gather(sems, place, size, sends):
        top = size // 2
        top -= top % 16
        spans = ((0, top), (top, size - top))
        lane = {"next": 0}

        def copy(origin_grp, origin_tp, span, device, slot):
            ref = place(origin_grp, origin_tp, span[0], span[1])
            return pltpu.make_async_remote_copy(
                src_ref=ref, dst_ref=ref, send_sem=a_send.at[sems, slot], recv_sem=a_recv.at[sems, slot],
                device_id=device, device_id_type=MESH)

        def send(g, s, span, device, slot):
            def described():
                return copy(lax.rem(my_grp + g, groups), tp_at(my_high - s + highs, my_low), span, device, slot)

            described().start()
            sends.append(described)

        def arrived(g, s, span, slot, low=None):
            low = my_low if low is None else low
            copy(lax.rem(my_grp + g, groups), tp_at(my_high - s + highs, low), span, x_next, slot).wait_recv()

        whole = (0, size)
        expected = []

        def to_sibling(g, s, span):
            if lows > 1:
                slot = lane["next"]
                lane["next"] += 1
                send(g, s, span, sibling, slot)
                expected.append((g, s, span, slot))

        x_slot = 5 * highs
        y_slot = x_slot + highs
        top_slot, low_slot = y_slot + 1, y_slot + 1 + highs

        def start():
            if highs > 1:
                send(0, 0, whole, x_next, x_slot)
            if groups > 1:
                send(0, 0, whole, across, y_slot)
            to_sibling(0, 0, whole)

        def turn():
            for s in range(1, highs):
                arrived(0, s, whole, x_slot + s - 1)
                if groups > 1:
                    send(0, s, spans[0], across, top_slot + s - 1)
                if s < highs - 1:
                    send(0, s, whole, x_next, x_slot + s)
                to_sibling(0, s, whole)
            if groups > 1:
                arrived(1, 0, whole, y_slot)
                if highs > 1:
                    send(1, 0, spans[1], x_next, low_slot)
                to_sibling(1, 0, whole)

        def finish():
            if groups > 1:
                for s in range(1, highs):
                    arrived(1, s, spans[1], low_slot + s - 1)
                    if s < highs - 1:
                        send(1, s, spans[1], x_next, low_slot + s)
                    to_sibling(1, s, spans[1])
                    arrived(1, s, spans[0], top_slot + s - 1)
                    to_sibling(1, s, spans[0])
            for g, s, span, slot in expected:
                arrived(g, s, span, slot, 1 - my_low)

        return start, turn, finish

    def token_gather(slot, sems, sends):
        return gather(sems, lambda g, t, offset, size: tokens_all.at[(slot,) + token_place(g, t, offset, size)],
                      rows, sends)

    def part_gather(index, part, halo, sends):
        size = rows + halo

        def place(g, t, offset, size_):
            return acts.at[index, pl.ds(part * size + offset, size_), columns_of(g, t)]

        return gather(2 + index * groups + part, place, size, sends)

    def normalize(x, layer):
        x = x.astype(jnp.float32)
        factor = lax.rsqrt(jnp.mean(x * x, axis=1, keepdims=True) + EPS)
        return (x * factor * gain[layer : layer + 1, :].astype(jnp.float32)).astype(jnp.bfloat16)

    def dot(a, b):
        return jnp.dot(a, b, preferred_element_type=jnp.float32)

    def project(x, first, g, at, size):
        gates[g, pl.ds(at, size), :] = dot(x, wide[first]).astype(jnp.bfloat16)
        inner_ = dot(x, wide[first + 1]).astype(jnp.bfloat16)
        values = dot(x, wide[first + 2]).astype(jnp.bfloat16)
        carried[g, pl.ds(PAD + at, size), :] = inner_.astype(jnp.float32) * values.astype(jnp.float32)

    def convolve(layer, g, at):
        conv = jnp.zeros((rows, width), jnp.float32)
        for tap in range(reach + 1):
            row = taps[layer, tap : tap + 1, own_columns].astype(jnp.float32)
            conv = conv + row * carried[g, PAD + at - reach + tap : PAD + at - reach + tap + rows, :]
        return (gates[g, at : at + rows, :].astype(jnp.float32) * conv).astype(jnp.bfloat16)

    def edge(layer, g):
        return pltpu.make_async_remote_copy(
            src_ref=edge_out.at[layer, g], dst_ref=edge_in.at[layer, g], send_sem=e_send.at[layer, g],
            recv_sem=e_recv.at[layer, g], device_id=right, device_id_type=MESH)

    def zero_edge(g, at):
        carried[g, PAD + at - reach : PAD + at, :] = jnp.zeros((reach, width), jnp.float32)

    def take_edge(layer, g, at):
        edge(layer, g).wait_recv()
        carried[g, PAD + at - reach : PAD + at, :] = edge_in[layer, g]

    def guest_mixed(g, slot):
        return pltpu.make_async_remote_copy(
            src_ref=mixed.at[g, pl.ds(pl.multiple_of(slot * rows, rows), rows), :],
            dst_ref=acts.at[0, pl.ds(g * rows, rows), own], send_sem=m_send.at[g], recv_sem=m_recv.at[g],
            device_id=outer, device_id_type=MESH)

    def later_layers(halo, ends, sends, going, need, hook):
        size = rows + halo
        first_size = chunk + halo
        spans = [(0, first_size)] + [(first_size + i * chunk, chunk) for i in range(rows // chunk - 1)]
        for layer in range(layers):
            index, first = 2 * layer, layer * KINDS
            top = layer == layers - 1
            coming = [None if top else part_gather(index + 1, g, halo, sends) for g in parts]
            for g in parts:
                hook(layer, "turn", g)
                going[g][1]()
            for g in parts:
                hook(layer, "finish", g)
                going[g][2]()
                need(first + 3)
                begin = halo if top else 0
                if not top:
                    for at, count in spans:
                        product = dot(acts[index, g * size + at : g * size + at + count, :], wide[first + 3])
                        stream = (resid[g, at : at + count, :].astype(jnp.float32) + product).astype(jnp.bfloat16)
                        resid[g, at : at + count, :] = stream
                        acts[index + 1, g * size + at : g * size + at + count, own] = stream
                    coming[g][0]()
                else:
                    @pl.loop(0, rows // chunk)
                    def _(c):
                        picked = pl.ds(pl.multiple_of(g * rows + c * chunk, chunk), chunk)
                        product = dot(acts[index, picked, :], wide[first + 3])
                        kept = resid[g, pl.ds(pl.multiple_of(halo + c * chunk, 8), chunk), :].astype(jnp.float32)
                        last[picked, :] = (kept + product).astype(jnp.bfloat16)
            if top:
                break
            for g in parts:
                hook(layer, "stream_turn", g)
                coming[g][1]()
            following = layer + 1
            first = following * KINDS
            going = [part_gather(2 * following, g, 0, sends) for g in parts]
            for g in parts:
                hook(layer, "stream_finish", g)
                coming[g][2]()
                for m in range(first, first + 3):
                    need(m)
                for i, (at, count) in enumerate(reversed(spans)):
                    x = acts[index + 1, g * size + at : g * size + at + count, :]
                    project(normalize(x, following), first, g, at, count)
                    if i == 0:
                        at_edge = PAD + size - reach
                        edge_out[following, g] = carried[g, at_edge : at_edge + reach, :]

                        @pl.when((me > 0) & (me < n - 1))
                        def _():
                            edge(following, g).start()
                if ends:
                    @pl.when(me == 0)
                    def _():
                        zero_edge(g, halo)

                @pl.when(me > 1)
                def _():
                    take_edge(following, g, halo)

                acts[2 * following, g * rows : (g + 1) * rows, own] = convolve(following, g, halo)
                going[g][0]()

        mine = pl.ds(pl.multiple_of(my_grp * rows, rows), rows)
        if groups > 1:
            other = lax.rem(my_grp + 1, groups)
            final = pltpu.make_async_remote_copy(
                src_ref=last.at[pl.ds(pl.multiple_of(other * rows, rows), rows), :], dst_ref=swap_in,
                send_sem=r_send, recv_sem=r_recv, device_id=across, device_id_type=MESH)
            final.start()
            result[:, own_columns] = last[mine, :]
            final.wait()
            result[:, pl.ds(pl.multiple_of(other * width, width), width)] = swap_in[...]
        else:
            result[...] = last[...]
        hook(layers, "last", 0)
        for c in sends:
            c().wait_send()

        @pl.when((me > 0) & (me < n - 1))
        def _():
            for layer in range(1, layers):
                for g in parts:
                    edge(layer, g).wait_send()

    assisted = range(3)
    rest = range(3, total)

    @pl.when(is_end)
    def _():
        sends = []
        away = pltpu.make_async_remote_copy(
            src_ref=tokens_all.at[(my_slot,) + token_place(my_grp, my_tp, 0, rows)],
            dst_ref=tokens_all.at[(my_slot,) + token_place(my_grp, my_tp, 0, rows)],
            send_sem=t_send.at[0], recv_sem=t_recv.at[0], device_id=inner, device_id_type=MESH)
        away.start()
        other = lax.rem(my_grp + 1, groups)

        def beside(g, columns_grp):
            ref = tokens_all.at[my_slot, pl.ds(pl.multiple_of(g * rows, rows), rows), columns_of(columns_grp, my_tp)]
            return pltpu.make_async_remote_copy(
                src_ref=ref, dst_ref=ref, send_sem=t_send.at[1], recv_sem=t_recv.at[1], device_id=across,
                device_id_type=MESH)

        if groups > 1:
            beside(my_grp, other).start()
        for m in range(total):
            if m >= 3:
                locals_[m + 1].wait()
            w_copy(m, me, 0).start()
        if groups > 1:
            beside(other, my_grp).wait_recv()
        for g in parts:
            resid[g, 0:rows, :] = tokens_all[my_slot, g * rows : (g + 1) * rows, own]
        going = [part_gather(0, g, 0, sends) for g in parts]
        for g in parts:
            guest_mixed(g, 0).wait_recv()
            going[g][0]()
        needed = set()

        def need(m):
            if m in needed:
                return
            needed.add(m)

            @pl.loop(1, n)
            def _(k):
                w_copy(m, me + step * k, 0).wait_recv()

        later_layers(0, True, sends, going, need, lambda *_: None)
        away.wait_send()
        if groups > 1:
            beside(my_grp, other).wait_send()
        for m in range(total):
            w_copy(m, me, 0).wait_send()

    @pl.when(jnp.logical_not(is_end))
    def _():
        sends = []

        def plain_or_rest(m):
            if m not in assisted:
                return True
            return False if helper is True else jnp.logical_not(helper)

        def own_in(m):
            w_copy(m, me, 0).start()

        def own_out(m):
            @when(plain_or_rest(m))
            def _():
                w_copy(m, me, 1).start()

        def every(limit, low, body):
            if isinstance(limit, int):
                for k in range(low, limit + 1):
                    body(k)
            else:
                for k in range(low, n - 1):
                    pl.when(k <= limit)(functools.partial(body, k))

        def event_out(m):
            def body(k):
                c = w_copy(m, me - step * k, 0)
                c.wait_recv()
                c.start()

            every(outer_max, 1, body)

        def event_in(m, low=1, high=None):
            def body(k):
                c = w_copy(m, me + step * k, 1)
                c.wait_recv()

                @when(plain_or_rest(m))
                def _():
                    c.start()

            every(inner_max if high is None else high, low, body)

        visitors = []
        guest_in = pltpu.make_async_remote_copy(
            src_ref=tokens_all.at[(guest_slot,) + token_place(my_grp, my_tp, 0, rows)],
            dst_ref=tokens_all.at[(guest_slot,) + token_place(my_grp, my_tp, 0, rows)],
            send_sem=t_send.at[0], recv_sem=t_recv.at[0], device_id=outer, device_id_type=MESH)
        start, turn, finish = token_gather(own_slot, 0, sends)
        g_start, g_turn, g_finish = token_gather(guest_slot, 1, visitors)

        def prepare(slot):
            @pl.loop(0, groups * rows // chunk)
            def _(c):
                picked = pl.ds(pl.multiple_of(c * chunk, chunk), chunk)
                normed[slot, picked, :] = normalize(tokens_all[slot, picked, :], 0)

        start()
        for m in assisted:
            own_in(m)
            own_out(m)
        for m in rest:
            locals_[m + 1].wait()
            own_out(m)
        turn()

        @when(helper)
        def _():
            guest_in.wait_recv()
            g_start()

        finish()
        event_out(0)
        for g in parts:
            resid[g, HALO : HALO + rows, :] = tokens_all[own_slot, g * rows : (g + 1) * rows, own]
        prepare(own_slot)
        event_out(1)
        when(helper)(g_turn)
        event_out(2)
        own_in(3)

        @when(helper)
        def _():
            g_finish()
            for g in parts:
                resid[g, 0:HALO, :] = tokens_all[guest_slot, (g + 1) * rows - HALO : (g + 1) * rows, own]
            prepare(guest_slot)

        if helper is not True:
            @pl.when(jnp.logical_not(helper))
            def _():
                for g in parts:
                    resid[g, 0:HALO, :] = jnp.zeros((HALO, width), jnp.bfloat16)
                    acts[0, g * (rows + HALO) : g * (rows + HALO) + HALO, own] = jnp.zeros((HALO, width), jnp.bfloat16)

        for m in assisted:
            event_in(m)
        event_out(3)
        own_in(4)

        going = [part_gather(0, g, HALO, sends) for g in parts]
        size = rows + HALO
        chunks = rows // chunk
        for g in parts:
            def run(slot, skip):
                @pl.loop(0, chunks)
                def _(i):
                    c = chunks - 1 - i
                    x = normed[slot, pl.ds(pl.multiple_of(g * rows + c * chunk, chunk), chunk), :]
                    project(x, 0, g, pl.multiple_of(slot * rows + c * chunk, chunk), chunk)

            def run_upper():
                run(1, 0)

            def run_lower():
                run(0, 0)

            def send_edge():
                at_edge = PAD + own_slot * rows + rows - 8
                edge_out[0, g] = carried[g, pl.ds(pl.multiple_of(at_edge, 8), 8), :][8 - reach :, :]

                @pl.when(me < n - 2)
                def _():
                    edge(0, g).start()

            when(helper)(run_upper)

            @pl.when(me == 1)
            def _():
                send_edge()

            run_lower()

            @pl.when(me != 1)
            def _():
                send_edge()

            @pl.when(me == 1)
            def _():
                zero_edge(g, 0)

            @pl.when(me > 1)
            def _():
                take_edge(0, g, 0)

            mixed[g, 0:rows, :] = convolve(0, g, 0)

            @when(helper)
            def _():
                mixed[g, rows : 2 * rows, :] = convolve(0, g, rows)
                acts[0, g * size : g * size + HALO, own] = mixed[
                    g, pl.ds(pl.multiple_of(guest_slot * rows + rows - HALO, HALO), HALO), :]
                guest_mixed(g, guest_slot).start()

            acts[0, g * size + HALO : (g + 1) * size, own] = mixed[
                g, pl.ds(pl.multiple_of(own_slot * rows, rows), rows), :]
            going[g][0]()

        tasks = [("o", 4), ("w", 5), ("i", 3), ("o", 5), ("w", 6), ("i", 4), ("o", 6), ("w", 7), ("i", 5), ("o", 7),
                 ("i", 6), ("i", 7)]
        assert total == 8
        points = {(0, "turn", 0): 2, (0, "turn", 1): 5, (0, "finish", 0): 5, (0, "finish", 1): 6,
                  (0, "stream_turn", 0): 8, (0, "stream_turn", 1): 9}

        def advance(count):
            while tasks and count > 0:
                kind, m = tasks.pop(0)
                {"o": event_out, "i": event_in, "w": own_in}[kind](m)
                count -= 1

        def hook(layer, what, g):
            done = 12 - len(tasks)
            if (layer, what, g) in points:
                advance(points[layer, what, g] - done)

        def need(m):
            while ("i", m) in tasks or ("o", m) in tasks:
                advance(1)

        later_layers(HALO, False, sends, going, need, hook)
        advance(12)

        @pl.when(me < n - 2)
        def _():
            for g in parts:
                edge(0, g).wait_send()

        @when(helper)
        def _():
            for c in visitors:
                c().wait_send()
            for g in parts:
                guest_mixed(g, guest_slot).wait_send()

        for m in range(total):
            w_copy(m, me, 0).wait_send()
            every(outer_max, 1, lambda k, m=m: w_copy(m, me - step * k, 0).wait_send())

            @when(plain_or_rest(m))
            def _(m=m):
                w_copy(m, me, 1).wait_send()
                every(inner_max, 1, lambda k: w_copy(m, me + step * k, 1).wait_send())


def shards(tokens, mix_gain, gate_weight, mix_weight, value_weight, out_weight, conv_taps):
    groups, n, tps = lax.axis_size("grp"), lax.axis_size("sp"), lax.axis_size("tp")
    assert groups <= 2 and n >= 4
    lows = 2 if tps % 2 == 0 else 1
    highs = tps // lows
    rows, block_width = tokens.shape
    layers, depth, _ = gate_weight.shape
    assert layers == 2
    reach = conv_taps.shape[1] - 1
    width = block_width // groups
    features = tps * block_width
    slots = 5 * highs + 3 * highs + 1
    total = layers * KINDS
    acts = 2 * layers - 1
    anywhere = pl.BlockSpec(memory_space=pl.ANY)
    vmem = pl.BlockSpec(memory_space=pltpu.VMEM)
    dma = pltpu.SemaphoreType.DMA
    return pl.pallas_call(
        functools.partial(kernel, (groups, n, tps, lows)),
        out_shape=jax.ShapeDtypeStruct(tokens.shape, tokens.dtype),
        in_specs=[anywhere, vmem, anywhere, anywhere, anywhere, anywhere, vmem],
        out_specs=vmem,
        scratch_shapes=[
            pltpu.VMEM((total, n * depth, width), jnp.bfloat16),
            pltpu.VMEM((acts, groups * (rows + HALO), features), jnp.bfloat16),
            pltpu.VMEM((2, groups * rows, features), jnp.bfloat16),
            pltpu.VMEM((2, groups * rows, features), jnp.bfloat16),
            pltpu.VMEM((groups, PAD + 2 * rows, width), jnp.float32),
            pltpu.VMEM((groups, 2 * rows, width), jnp.bfloat16),
            pltpu.VMEM((groups, 2 * rows, width), jnp.bfloat16),
            pltpu.VMEM((groups, rows + HALO, width), jnp.bfloat16),
            pltpu.VMEM((layers, groups, reach, width), jnp.float32),
            pltpu.VMEM((layers, groups, reach, width), jnp.float32),
            pltpu.VMEM((groups * rows, width), jnp.bfloat16),
            pltpu.VMEM((rows, width), jnp.bfloat16),
            dma((total + 1,)),
            dma((total, 2, n)),
            dma((total, n)),
            dma((2 + acts * groups, slots)),
            dma((2 + acts * groups, slots)),
            dma((layers, groups)),
            dma((layers, groups)),
            dma,
            dma,
            dma((2,)),
            dma((2,)),
            dma((groups,)),
            dma((groups,)),
        ],
        compiler_params=pltpu.CompilerParams(
            collective_id=0, has_side_effects=True, vmem_limit_bytes=60 * 1024 * 1024
        ),
        name="mixers",
    )(tokens, mix_gain, gate_weight, mix_weight, value_weight, out_weight, conv_taps)


def solution(mesh):
    return jax.shard_map(
        shards,
        mesh=mesh,
        in_specs=(
            P(("grp", "sp"), "tp"),
            P(),
            P(None, "sp", "tp"),
            P(None, "sp", "tp"),
            P(None, "sp", "tp"),
            P(None, "sp", "tp"),
            P(None, None, "tp"),
        ),
        out_specs=P(("grp", "sp"), "tp"),
        check_vma=False,
    )
```

time: 169 us -> 157 us (0.929)
  the two profiles are of different devices: /device:TPU:0 before, /device:TPU:25 now
where the time goes in v1:
time: 157 us
  Pallas kernels  154 us (98%)
  local copies, waits for them, and re-layouts  3.16 us (2%)
    pallas_call x1, Pallas kernels, shards(): pl.pallas_call(functools.partial(kernel, (groups, n, tps, lows)), out_sha...  154 us
    unnamed x2, local copies, waits for them, and re-layouts  3.16 us

profile of v1, /device:TPU:25, one launch (start us, length us, event | category | flops | bytes accessed | tf_op | source)
XLA Modules:
  0.0 156.8 jit_solution(16997841010120003059)
XLA Ops:
  0.0 1.3 copy.8.taps
  1.3 153.6 %mixers.1 = bf16[512,512]{1,0:T(8,128)(2,1)} custom-call(bf16[512,512]{1,0:T(8,128)(2,1)} %tokens.1, bf16[2,2048]{1,0:T(2,128)(2,1)} %gain.1, bf16[2,512,512]{2,1,0:T(8,128)(2,1)} %gate_w.1, bf16[2,512,512]{2,1,0:T(8,128)(2,1)} %mix_w.1, bf16[2,512,512]{2,1,0:T(8,128)(2,1)} %value_w.1, bf16[2,512,512]{2,1,0:T(8,128)(2,1)} %out_w.1, bf16[2,3,512]{2,1,0:T(4,128)(2,1)} %copy.8.taps), custom_call_target="tpu_custom_call" | custom-call | tf_op jit(solution)/shard_map/mixers/pallas_call | solution.py:597
  154.9 1.9 %copy.10 = bf16[512,512]{1,0:T(8,128)(2,1)} copy(bf16[512,512]{1,0:T(8,128)(2,1)} %mixers.1) | data formatting | bytes 1048576

commit v2 on v1

v2 whole, which is shorter than its diff:
```python
import functools

import jax
import jax.numpy as jnp
from jax import lax
from jax.experimental import pallas as pl
from jax.experimental.pallas import tpu as pltpu
from jax.sharding import PartitionSpec as P

EPS = 1e-06
KINDS = 4
HALO = 16
PAD = 8
MESH = pl.DeviceIdType.MESH
scope = jax.named_scope


def when(condition):
    if condition is True:
        return lambda body: body()
    if condition is False:
        return lambda body: None
    return pl.when(condition)


def gather_sems(highs, fine):
    return 8 * (highs - 1) + 5 if fine else 6 * (highs - 1) + 3


def kernel(sizes, tokens, gain, gate_w, mix_w, value_w, out_w, taps, result,
           wide, acts, deep, tokens_all, halo_all, normed, carried, gates, mixed, resid, last, swap_in,
           local_sem, w_send, w_recv, a_send, a_recv, r_send, r_recv, t_send, t_recv, m_send, m_recv):
    groups, n, tps, lows, gathers, cuts, reach = sizes
    highs = tps // lows
    rows, block_width = tokens.shape
    layers = gate_w.shape[0]
    depth = gate_w.shape[1]
    width = block_width // groups
    half = width // cuts
    total = layers * KINDS
    final_first = total - KINDS
    fine = range(3)
    pieces = [(m, low, half if m in fine else width)
              for m in range(total) for low in range(0, width, half if m in fine else width)]
    lines = len(pieces)

    def line_of(m, cut=0):
        return pieces.index((m, cut * half, half if m in fine else width))

    chunk = min(rows, 256)
    parts = range(groups)
    me, my_grp, my_tp = lax.axis_index("sp"), lax.axis_index("grp"), lax.axis_index("tp")
    my_high, my_low = my_tp // lows, lax.rem(my_tp, lows)

    def tp_at(high, low):
        return lax.rem(high + highs, highs) * lows + low

    x_next, x_prev = {"tp": tp_at(my_high + 1, my_low)}, {"tp": tp_at(my_high - 1 + highs, my_low)}
    across = {"grp": lax.rem(my_grp + 1, groups)}
    sibling = {"tp": my_high * lows + (1 - my_low)}
    right, left = {"sp": me + 1}, {"sp": me - 1}

    lower = 2 * me < n
    step = jnp.where(lower, 1, -1)
    inner, outer = {"sp": me + step}, {"sp": me - step}
    is_end = (me == 0) | (me == n - 1)
    helper = True if n == 4 else (me == 1) | (me == n - 2)
    outer_max = 1 if n == 4 else jnp.where(lower, me, n - 1 - me)
    inner_max = n - 1 - outer_max

    barrier = pltpu.get_barrier_semaphore()
    fixed = []
    if highs > 1:
        fixed.append(x_next)
    if highs > 2:
        fixed.append(x_prev)
    if groups > 1:
        fixed.append(across)
    if lows > 1:
        fixed.append(sibling)
    for device in fixed:
        pl.semaphore_signal(barrier, inc=1, device_id=device, device_id_type=MESH)

    @pl.when(me > 0)
    def _():
        pl.semaphore_signal(barrier, inc=1, device_id=left, device_id_type=MESH)

    @pl.when(me < n - 1)
    def _():
        pl.semaphore_signal(barrier, inc=1, device_id=right, device_id_type=MESH)

    weights = (gate_w, mix_w, value_w, out_w)
    own_columns = pl.ds(pl.multiple_of(my_grp * width, width), width)

    def w_rows(origin):
        return pl.ds(pl.multiple_of(origin * depth, depth), depth)

    def token_place(g, t, offset, size):
        return (pl.ds(pl.multiple_of(g * rows + offset, 8), size),
                pl.ds(pl.multiple_of(t * block_width, block_width), block_width))

    def columns_of(g, t):
        return pl.ds(pl.multiple_of(t * block_width + g * width, width), width)

    own = columns_of(my_grp, my_tp)
    own_slot = jnp.where(me == 1, 1, 0)
    guest_slot = 1 - own_slot
    my_slot = jnp.where(is_end, jnp.where(me == 0, 0, 1), own_slot)

    locals_ = [pltpu.make_async_copy(
        tokens, tokens_all.at[(my_slot,) + token_place(my_grp, my_tp, 0, rows)], local_sem.at[0])]
    loads = [[] for _ in range(total)]
    for m in range(total):
        if final_first <= m < final_first + 3:
            continue
        loads[m].append(pltpu.make_async_copy(
            weights[m % KINDS].at[m // KINDS, :, own_columns], wide.at[m, w_rows(me), :], local_sem.at[m + 1]))
    for piece in range(3 * cuts):
        m, at = final_first + piece // cuts, piece % cuts * half
        source = pl.ds(pl.multiple_of(my_grp * width + piece // 3 * half, half), half)
        loads[m].append(pltpu.make_async_copy(
            weights[piece % 3].at[layers - 1, :, source], wide.at[m, w_rows(me), pl.ds(at, half)],
            local_sem.at[total + 1 + piece]))
    locals_[0].start()
    for copies in loads:
        for copy in copies:
            copy.start()

    def loaded(m):
        for copy in loads[m]:
            copy.wait()

    with scope("loads"):
        locals_[0].wait()
        for m in range(3):
            loaded(m)

    with scope("entry"):
        pl.semaphore_wait(barrier, len(fixed) + jnp.minimum(me, 1) + jnp.minimum(n - 1 - me, 1))

    def w_copy(m, origin, way):
        matrix, low, columns = pieces[m]
        ref = wide.at[matrix, w_rows(origin), low : low + columns]
        return pltpu.make_async_remote_copy(
            src_ref=ref, dst_ref=ref, send_sem=w_send.at[m, way, origin], recv_sem=w_recv.at[m, origin],
            device_id=inner if way == 0 else outer, device_id_type=MESH)

    sem_bases = [0]
    for index in range(gathers):
        sem_bases.append(sem_bases[-1] + gather_sems(highs, index != 2 and index < 3 + 2 * groups))

    def gather(sems, place, size, sends, fine=False):
        top = size // 2
        top = size if size < 64 else top - top % 16
        spans = ((0, top), (top, size - top))
        split = top < size
        whole = (0, size)
        slots = {}

        def slot_of(key):
            return sem_bases[sems] + slots.setdefault(key, len(slots))

        def copy(origin_grp, origin_tp, span, device, key):
            ref = place(origin_grp, origin_tp, span[0], span[1])
            return pltpu.make_async_remote_copy(
                src_ref=ref, dst_ref=ref, send_sem=a_send.at[slot_of(key)], recv_sem=a_recv.at[slot_of(key)],
                device_id=device, device_id_type=MESH)

        def send(g, s, span, device, key):
            def described():
                return copy(lax.rem(my_grp + g, groups), tp_at(my_high - s + highs, my_low), span, device, key)

            described().start()
            sends.append(described)

        def arrived(g, s, span, key, low=None):
            low = my_low if low is None else low
            copy(lax.rem(my_grp + g, groups), tp_at(my_high - s + highs, low), span, x_next, key).wait_recv()

        expected = []

        def to_sibling(g, s, span):
            if lows > 1:
                key = ("sibling", len(expected))
                send(g, s, span, sibling, key)
                expected.append((g, s, span, key))

        x_spans = ((0, spans[0]), (1, spans[1])) if fine else ((0, whole),)
        y_spans = ((1, spans[1]), (0, spans[0])) if fine else ((1, whole),)

        def start():
            for i, span in x_spans:
                if highs > 1:
                    send(0, 0, span, x_next, ("x", 0, i))
            for i, span in y_spans:
                if groups > 1:
                    send(0, 0, span, across, ("y", i))
            to_sibling(0, 0, whole)

        def turn_one(which):
            for s in range(1, highs):
                for i, span in x_spans[which]:
                    arrived(0, s, span, ("x", s - 1, i))
                    if groups > 1 and i == 0:
                        send(0, s, spans[0], across, ("top", s - 1))
                    if s < highs - 1:
                        send(0, s, span, x_next, ("x", s, i))
                    to_sibling(0, s, span)
            if groups > 1:
                for i, span in y_spans[which]:
                    arrived(1, 0, span, ("y", i))
                    if highs > 1 and split and i == 1:
                        send(1, 0, spans[1], x_next, ("low", 0))
                    to_sibling(1, 0, span)

        def turn_first():
            turn_one(slice(0, 1))

        def turn_second():
            turn_one(slice(1, 2))

        def turn():
            turn_first()
            turn_second()

        def finish():
            if groups > 1:
                for s in range(1, highs):
                    if split:
                        arrived(1, s, spans[1], ("low", s - 1))
                        if s < highs - 1:
                            send(1, s, spans[1], x_next, ("low", s))
                        to_sibling(1, s, spans[1])
                    arrived(1, s, spans[0], ("top", s - 1))
                    to_sibling(1, s, spans[0])
            for g, s, span, key in expected:
                arrived(g, s, span, key, 1 - my_low)
            assert len(slots) <= sem_bases[sems + 1] - sem_bases[sems]

        return start, turn, finish, turn_first, turn_second

    def token_gather(slot, sems, sends):
        return gather(sems, lambda g, t, offset, size: tokens_all.at[(slot,) + token_place(g, t, offset, size)],
                      rows, sends, True)

    def halo_gather(sends):
        def place(g, t, offset, size):
            return halo_all.at[pl.ds(pl.multiple_of(g * HALO + offset, HALO), size), token_place(g, t, 0, HALO)[1]]

        return gather(2, place, HALO, sends)

    def cut_columns(g, t, cut):
        return pl.ds(pl.multiple_of(t * block_width + g * width + cut * half, half), half)

    block = rows // groups

    def part_gather(index, part, sends):
        size = rows + HALO

        def place(g, t, offset, size_):
            return acts.at[index, pl.ds(part * size + offset, size_), columns_of(g, t)]

        return gather(3 + index * groups + part, place, size, sends, True)

    def deep_gather(cut, part, sends):
        def place(g, t, offset, size):
            if cut < cuts - 1:
                return deep.at[part, pl.ds(offset, size), cut_columns(g, t, cut)]
            return deep.at[:, pl.ds(part * block + offset, size), cut_columns(g, t, cut)]

        return gather(3 + (2 + cut) * groups + part, place, rows if cut < cuts - 1 else block, sends)

    def normalize(x, layer):
        x = x.astype(jnp.float32)
        factor = lax.rsqrt(jnp.mean(x * x, axis=1, keepdims=True) + EPS)
        return (x * factor * gain[layer : layer + 1, :].astype(jnp.float32)).astype(jnp.bfloat16)

    def dot(a, b):
        return jnp.dot(a, b, preferred_element_type=jnp.float32)

    def project(x, first, g, at, size):
        gates[g, pl.ds(at, size), :] = dot(x, wide[first]).astype(jnp.bfloat16)
        inner_ = dot(x, wide[first + 1]).astype(jnp.bfloat16)
        values = dot(x, wide[first + 2]).astype(jnp.bfloat16)
        carried[g, pl.ds(PAD + at, size), :] = inner_.astype(jnp.float32) * values.astype(jnp.float32)

    def project_first(x, g, at, size):
        if cuts == 1:
            project(x, final_first, g, at, size)
            return
        early = dot(x, wide[final_first]).astype(jnp.bfloat16)
        later = dot(x, wide[final_first + 1]).astype(jnp.bfloat16)
        gates[g, at : at + size, 0:half] = early[:, :half]
        gates[g, at : at + size, half:] = later[:, half:]
        carried[g, PAD + at : PAD + at + size, 0:half] = (
            early[:, half:].astype(jnp.float32) * later[:, :half].astype(jnp.float32))

    def project_second(x, g, at, size):
        both = dot(x, wide[final_first + 2]).astype(jnp.bfloat16)
        carried[g, PAD + at : PAD + at + size, half:] = (
            both[:, :half].astype(jnp.float32) * both[:, half:].astype(jnp.float32))

    def convolve(layer, g, at, size, low, count):
        conv = jnp.zeros((size, count), jnp.float32)
        for tap in range(reach + 1):
            picked = pl.ds(pl.multiple_of(my_grp * width + low, 128), count)
            row = taps[tap, layer : layer + 1, picked].astype(jnp.float32)
            begin = PAD + at - reach + tap
            conv = conv + row * carried[g, begin : begin + size, low : low + count]
        return (gates[g, at : at + size, low : low + count].astype(jnp.float32) * conv).astype(jnp.bfloat16)

    guest_spans = [(0, chunk + HALO)] + [(HALO + i * chunk, chunk) for i in range(1, rows // chunk)]

    def guest_mixed(g, slot, i):
        at, length = guest_spans[i]
        return pltpu.make_async_remote_copy(
            src_ref=mixed.at[g, pl.ds(pl.multiple_of(slot * rows + at, HALO), length), :],
            dst_ref=acts.at[0, pl.ds(g * (HALO + rows) + at, length), own], send_sem=m_send.at[g, i],
            recv_sem=m_recv.at[g, i], device_id=outer, device_id_type=MESH)

    halo_kept = pltpu.make_async_remote_copy(
        src_ref=resid.at[:, rows : rows + HALO, :], dst_ref=resid.at[:, 0:HALO, :], send_sem=t_send.at[3],
        recv_sem=t_recv.at[3], device_id=right, device_id_type=MESH)

    def later_layers(sends, going, need, hook, eager):
        size = rows + HALO
        spans = [(0, chunk + HALO)] + [(HALO + i * chunk, chunk) for i in range(1, rows // chunk)]
        coming = [part_gather(1, g, sends) for g in parts]
        def second_hop(g):
            hook("turn", g)
            with scope(f"turn0_{g}"):
                if g > 0:
                    going[g][3]()
                going[g][4]()

        if not eager:
            for g in parts:
                second_hop(g)
        for g in parts:
            hook("finish", g)
            if eager and g == 0:
                second_hop(g)
            with scope(f"finish0_{g}"):
                going[g][2]()
            if eager and g < groups - 1:
                second_hop(g + 1)
            with scope(f"need0_{g}"):
                need(line_of(3))
            for at, count in spans:
                product = dot(acts[0, g * size + at : g * size + at + count, :], wide[3])
                stream = (resid[g, at : at + count, :].astype(jnp.float32) + product).astype(jnp.bfloat16)
                resid[g, at : at + count, :] = stream
                acts[1, g * size + at : g * size + at + count, own] = stream
            coming[g][0]()
        for g in parts:
            hook("stream_turn", g)
            with scope(f"sturn{g}"):
                coming[g][1]()

        going = {(cut, g): deep_gather(cut, g, sends) for cut in range(cuts) for g in parts}

        def fill(cut, g):
            deep[g, :, cut_columns(my_grp, my_tp, cut)] = convolve(layers - 1, g, HALO, rows, cut * half, half)

        for g in parts:
            hook("stream_finish", g)
            with scope(f"sfinish{g}"):
                coming[g][2]()
            for at, count in spans:
                normed[g, at : at + count, :] = normalize(acts[1, g * size + at : g * size + at + count, :], layers - 1)
            with scope(f"sneed{g}"):
                for m in range(final_first, final_first + (2 if cuts == 2 else 3)):
                    need(line_of(m))
            with scope(f"first{g}"):
                for at, count in spans:
                    project_first(normed[g, at : at + count, :], g, at, count)
                fill(0, g)
            if cuts == 2:
                going[0, g][0]()
        if cuts == 2:
            for g in parts:
                hook("first_turn", g)
                with scope(f"turn1_{g}"):
                    going[0, g][1]()
            hook("second", 0)
            with scope("vneed"):
                need(line_of(final_first + 2))
            with scope("second"):
                for g in parts:
                    for at, count in spans:
                        project_second(normed[g, at : at + count, :], g, at, count)
                    fill(1, g)
        for u in parts:
            going[cuts - 1, u][0]()
        for g in parts:
            hook("second_turn", g)
            with scope(f"turn2_{g}"):
                going[cuts - 1, g][1]()
        if cuts == 2:
            for g in parts:
                with scope(f"finish1_{g}"):
                    going[0, g][2]()

        other = lax.rem(my_grp + 1, groups)
        writes, swaps = [], []
        flushed = 0
        for u in parts:
            hook("second_finish", u)
            with scope(f"finish2_{u}"):
                going[cuts - 1, u][2]()
            with scope(f"oneed{u}"):
                need(line_of(total - 1))
            for group, at in (((other, 0),) if groups > 1 else ()) + ((my_grp, groups - 1),):
                product = dot(deep[group, u * block : (u + 1) * block, :], wide[total - 1])
                kept = resid[group, HALO + u * block : HALO + (u + 1) * block, :].astype(jnp.float32)
                last[at, u] = (kept + product).astype(jnp.bfloat16)
                if groups > 1 and at == 0:
                    swap = pltpu.make_async_remote_copy(
                        src_ref=last.at[0, u], dst_ref=swap_in.at[u], send_sem=r_send.at[u],
                        recv_sem=r_recv.at[u], device_id=across, device_id_type=MESH)
                    swap.start()
                    swaps.append(swap)
            lines_of = pl.ds(u * block, block)
            writes.append(pltpu.make_async_copy(
                last.at[groups - 1, u], result.at[lines_of, own_columns], local_sem.at[total + 1 + 3 * cuts + u]))
            writes[-1].start()
            if u == 0:
                with scope("flush"):
                    flushed = len(sends) // 2
                    for c in sends[:flushed]:
                        c().wait_send()
        with scope("flush"):
            for c in sends[flushed:]:
                c().wait_send()
        for u, swap in enumerate(swaps):
            with scope(f"swap{u}"):
                swap.wait_recv()
            columns = pl.ds(pl.multiple_of(other * width, width), width)
            writes.append(pltpu.make_async_copy(
                swap_in.at[u], result.at[pl.ds(u * block, block), columns],
                local_sem.at[total + 1 + 3 * cuts + groups + u]))
            writes[-1].start()
        hook("last", 0)
        with scope("writes"):
            for swap in swaps:
                swap.wait_send()
            for write in writes:
                write.wait()

    assisted = range(3 * cuts)
    rest = range(3 * cuts, lines)

    @pl.when(is_end)
    def _():
        sends = []
        away = pltpu.make_async_remote_copy(
            src_ref=tokens_all.at[(my_slot,) + token_place(my_grp, my_tp, 0, rows)],
            dst_ref=tokens_all.at[(my_slot,) + token_place(my_grp, my_tp, 0, rows)],
            send_sem=t_send.at[0], recv_sem=t_recv.at[0], device_id=inner, device_id_type=MESH)
        away.start()
        other = lax.rem(my_grp + 1, groups)

        def beside(g, columns_grp):
            ref = tokens_all.at[my_slot, pl.ds(pl.multiple_of(g * rows, rows), rows), columns_of(columns_grp, my_tp)]
            return pltpu.make_async_remote_copy(
                src_ref=ref, dst_ref=ref, send_sem=t_send.at[1], recv_sem=t_recv.at[1], device_id=across,
                device_id_type=MESH)

        if groups > 1:
            beside(my_grp, other).start()
        for m in range(lines):
            if pieces[m][0] >= 3 and pieces[m][1] == 0:
                loaded(pieces[m][0])
            w_copy(m, me, 0).start()
        if groups > 1:
            beside(other, my_grp).wait_recv()
        for g in parts:
            resid[g, HALO : HALO + rows, :] = tokens_all[my_slot, g * rows : (g + 1) * rows, own]

        @pl.when(me == 0)
        def _():
            resid[:, 0:HALO, :] = jnp.zeros((groups, HALO, width), jnp.bfloat16)

        @pl.when(me > 0)
        def _():
            halo_kept.wait_recv()

        going = [part_gather(0, g, sends) for g in parts]
        for g in parts:
            with scope(f"back_{g}"):
                for i in range(len(guest_spans)):
                    guest_mixed(g, 0, i).wait_recv()
            going[g][0]()
            if g == 0:
                going[g][3]()
        needed = set()

        def need(m):
            if m in needed:
                return
            needed.add(m)

            @pl.loop(1, n)
            def _(k):
                w_copy(m, me + step * k, 0).wait_recv()

        later_layers(sends, going, need, lambda *_: None, True)
        away.wait_send()
        if groups > 1:
            beside(my_grp, other).wait_send()
        for m in range(lines):
            w_copy(m, me, 0).wait_send()

    @pl.when(jnp.logical_not(is_end))
    def _():
        sends = []

        def plain_or_rest(m):
            if m not in assisted:
                return True
            return False if helper is True else jnp.logical_not(helper)

        def own_in(m):
            w_copy(m, me, 0).start()

        def own_out(m):
            @when(plain_or_rest(m))
            def _():
                w_copy(m, me, 1).start()

        def every(limit, low, body):
            if isinstance(limit, int):
                for k in range(low, limit + 1):
                    body(k)
            else:
                for k in range(low, n - 1):
                    pl.when(k <= limit)(functools.partial(body, k))

        def event_out(m):
            def body(k):
                c = w_copy(m, me - step * k, 0)
                with scope(f"o{m}"):
                    c.wait_recv()
                c.start()

            every(outer_max, 1, body)

        def event_in(m, low=1, high=None):
            def body(k):
                c = w_copy(m, me + step * k, 1)
                with scope(f"i{m}_{k}"):
                    c.wait_recv()

                @when(plain_or_rest(m))
                def _():
                    c.start()

            every(inner_max if high is None else high, low, body)

        visitors = []
        guest_in = pltpu.make_async_remote_copy(
            src_ref=tokens_all.at[(guest_slot,) + token_place(my_grp, my_tp, 0, rows)],
            dst_ref=tokens_all.at[(guest_slot,) + token_place(my_grp, my_tp, 0, rows)],
            send_sem=t_send.at[0], recv_sem=t_recv.at[0], device_id=outer, device_id_type=MESH)
        start, turn, finish, _, _ = token_gather(own_slot, 0, sends)
        g_start, _, g_finish, g_turn_first, g_turn_second = token_gather(guest_slot, 1, visitors)

        def prepare(slot):
            for g in parts:
                @pl.loop(0, rows // chunk)
                def _(c):
                    x = tokens_all[slot, pl.ds(pl.multiple_of(g * rows + c * chunk, chunk), chunk), :]
                    normed[g, pl.ds(pl.multiple_of(HALO + slot * rows + c * chunk, HALO), chunk), :] = normalize(x, 0)

        mates = []
        h_start, h_turn, h_finish, _, _ = halo_gather(mates)
        halo_there = (pl.ds(pl.multiple_of(my_grp * HALO, HALO), HALO), token_place(my_grp, my_tp, 0, rows)[1])
        halo_out = pltpu.make_async_remote_copy(
            src_ref=tokens_all.at[(own_slot,) + token_place(my_grp, my_tp, rows - HALO, HALO)],
            dst_ref=halo_all.at[halo_there], send_sem=t_send.at[2], recv_sem=t_recv.at[2], device_id=right,
            device_id_type=MESH)

        @pl.when(me < n - 2)
        def _():
            halo_out.start()

        start()
        for m in assisted:
            own_in(m)
            own_out(m)
        for m in rest:
            if pieces[m][1] == 0:
                loaded(pieces[m][0])
            own_out(m)

        @pl.when(me > 1)
        def _():
            halo_out.wait_recv()
            h_start()

        for g in parts:
            carried[g, 0:PAD, :] = jnp.zeros((PAD, width), jnp.float32)

        with scope("tturn"):
            turn()

        @pl.when(me > 1)
        def _():
            h_turn()

        @when(helper)
        def _():
            with scope("guest"):
                guest_in.wait_recv()
            g_start()

        event_out(line_of(0, 0))
        if cuts == 2:
            event_out(line_of(0, 1))
        with scope("tfinish"):
            finish()
        for g in parts:
            resid[g, HALO : HALO + rows, :] = tokens_all[own_slot, g * rows : (g + 1) * rows, own]
        event_out(line_of(1, 0))

        @pl.when(me > 1)
        def _():
            h_finish()
            for g in parts:
                resid[g, 0:HALO, :] = halo_all[g * HALO : (g + 1) * HALO, own]
                normed[g, 0:HALO, :] = normalize(halo_all[g * HALO : (g + 1) * HALO, :], 0)

        @pl.when(me == 1)
        def _():
            for g in parts:
                normed[g, 0:HALO, :] = jnp.zeros((HALO, normed.shape[2]), jnp.bfloat16)

        with scope("prepare"):
            prepare(own_slot)
        if cuts == 2:
            event_out(line_of(1, 1))
        with scope("gturn"):
            when(helper)(g_turn_first)
        event_out(line_of(2, 0))
        if cuts == 2:
            event_out(line_of(2, 1))
        own_in(line_of(3))
        with scope("gturn"):
            when(helper)(g_turn_second)
        @pl.when(me == n - 2)
        def _():
            halo_kept.start()

        for m in assisted[: 2 * len(assisted) // 3]:
            event_in(m)

        @when(helper)
        def _():
            with scope("gfinish"):
                g_finish()
            with scope("gprepare"):
                prepare(guest_slot)

        for m in assisted[2 * len(assisted) // 3 :]:
            event_in(m)

        @pl.when(me == 1)
        def _():
            for g in parts:
                resid[g, 0:HALO, :] = tokens_all[0, (g + 1) * rows - HALO : (g + 1) * rows, own]

        going = [part_gather(0, g, sends) for g in parts]
        size = rows + HALO
        firsts = [(0, chunk + HALO)] + [(HALO + i * chunk, chunk) for i in range(1, rows // chunk)]
        seconds = [(size + i * chunk, chunk) for i in range(rows // chunk)]

        def run(g, spans, low, high):
            for at, length in spans:
                project(normed[g, at : at + length, :], 0, g, at, length)
            mixed[g, low:high, :] = convolve(0, g, low, high - low, 0, width)

        for g in parts:
            for i, (at, length) in enumerate(guest_spans):
                with scope(f"guests{g}"):
                    @pl.when(me == 1)
                    def _():
                        run(g, [(at, length)], at, at + length)

                    @pl.when(me == n - 2)
                    def _():
                        before = firsts[-1:] if i == 0 else []
                        run(g, before + seconds[i : i + 1], rows + at, rows + at + length)

                @when(helper)
                def _():
                    guest_mixed(g, guest_slot, i).start()

        event_out(line_of(3))
        own_in(line_of(4))
        for g in parts:
            with scope(f"owns{g}"):
                @pl.when(me == 1)
                def _():
                    run(g, seconds, size, size + rows)

                @pl.when(me == n - 2)
                def _():
                    run(g, firsts[:-1], 0, rows)

                if n > 4:
                    @pl.when(jnp.logical_not(helper))
                    def _():
                        run(g, firsts, 0, size)

            acts[0, g * size : (g + 1) * size, own] = mixed[
                g, pl.ds(pl.multiple_of(own_slot * rows, rows), size), :]
            going[g][0]()
            if g == groups - 1:
                going[0][3]()

        p = [line_of(m) for m in range(total)]
        order = [("turn", 0, [("o", p[4]), ("w", p[5]), ("i", p[3], 1)]),
                 ("turn", 1, [("o", p[5]), ("w", p[6]), ("i", p[3], 2)]),
                 ("finish", 0, [("o", p[6]), ("w", p[7]), ("i", p[4], 1)]),
                 ("finish", 1, [("o", p[7]), ("i", p[4], 2)]),
                 ("stream_turn", 0, [("i", p[5], 1)]),
                 ("stream_turn", 1, [("i", p[5], 2)]),
                 ("stream_finish", 0, [("i", p[6], 1)]),
                 ("stream_finish", 1, [("i", p[6], 2)]),
                 ("second", 0, [("i", p[7], 1)]),
                 ("first_turn", 1, [("i", p[7], 2)])]
        assert total == 8
        points = {}
        tasks = []
        for what, g, some in order:
            tasks += some
            if some:
                points[what, g] = some[-1]

        def pass_on(kind, m, k=None):
            if kind == "i" and k == 1:
                event_in(m, 1, 1)
            elif kind == "i":
                event_in(m, 2)
            else:
                {"o": event_out, "w": own_in}[kind](m)

        def hook(what, g):
            if (what, g) in points:
                while points[what, g] in tasks:
                    pass_on(*tasks.pop(0))

        def need(m):
            while any(task[1] == m for task in tasks):
                pass_on(*tasks.pop(0))

        @pl.when(me == n - 2)
        def _():
            halo_kept.wait_send()

        later_layers(sends, going, need, hook, False)
        while tasks:
            pass_on(*tasks.pop(0))

        @pl.when(me < n - 2)
        def _():
            halo_out.wait_send()


        @pl.when(me > 1)
        def _():
            for c in mates:
                c().wait_send()

        @when(helper)
        def _():
            for c in visitors:
                c().wait_send()
            for g in parts:
                for i in range(len(guest_spans)):
                    guest_mixed(g, guest_slot, i).wait_send()

        for m in range(lines):
            w_copy(m, me, 0).wait_send()
            every(outer_max, 1, lambda k, m=m: w_copy(m, me - step * k, 0).wait_send())

            @when(plain_or_rest(m))
            def _(m=m):
                w_copy(m, me, 1).wait_send()
                every(inner_max, 1, lambda k: w_copy(m, me + step * k, 1).wait_send())


def shards(tokens, mix_gain, gate_weight, mix_weight, value_weight, out_weight, conv_taps):
    groups, n, tps = lax.axis_size("grp"), lax.axis_size("sp"), lax.axis_size("tp")
    assert groups <= 2 and n >= 4
    lows = 2 if tps % 2 == 0 else 1
    highs = tps // lows
    rows, block_width = tokens.shape
    layers, depth, _ = gate_weight.shape
    assert layers == 2
    reach = conv_taps.shape[1] - 1
    width = block_width // groups
    features = tps * block_width
    total = layers * KINDS
    acts = 2 * layers - 2
    cuts = 2 if width % 256 == 0 else 1
    pieces = total + 3 * (cuts - 1)
    gathers = 3 + (acts + cuts) * groups
    slots = sum(gather_sems(highs, index != 2 and index < 3 + 2 * groups) for index in range(gathers))
    anywhere = pl.BlockSpec(memory_space=pl.ANY)
    vmem = pl.BlockSpec(memory_space=pltpu.VMEM)
    dma = pltpu.SemaphoreType.DMA
    return pl.pallas_call(
        functools.partial(kernel, (groups, n, tps, lows, gathers, cuts, reach)),
        out_shape=jax.ShapeDtypeStruct(tokens.shape, tokens.dtype),
        in_specs=[anywhere, vmem, anywhere, anywhere, anywhere, anywhere, vmem],
        out_specs=anywhere,
        scratch_shapes=[
            pltpu.VMEM((total, n * depth, width), jnp.bfloat16),
            pltpu.VMEM((acts, groups * (rows + HALO), features), jnp.bfloat16),
            pltpu.VMEM((groups, rows, features), jnp.bfloat16),
            pltpu.VMEM((2, groups * rows, features), jnp.bfloat16),
            pltpu.VMEM((groups * HALO, features), jnp.bfloat16),
            pltpu.VMEM((groups, HALO + 2 * rows, features), jnp.bfloat16),
            pltpu.VMEM((groups, PAD + HALO + 2 * rows, width), jnp.float32),
            pltpu.VMEM((groups, HALO + 2 * rows, width), jnp.bfloat16),
            pltpu.VMEM((groups, HALO + 2 * rows, width), jnp.bfloat16),
            pltpu.VMEM((groups, rows + HALO, width), jnp.bfloat16),
            pltpu.VMEM((groups, groups, rows // groups, width), jnp.bfloat16),
            pltpu.VMEM((groups, rows // groups, width), jnp.bfloat16),
            dma((total + 1 + 3 * cuts + 2 * groups,)),
            dma((pieces, 2, n)),
            dma((pieces, n)),
            dma((slots,)),
            dma((slots,)),
            dma((groups,)),
            dma((groups,)),
            dma((4,)),
            dma((4,)),
            dma((groups, max(rows // 256, 1))),
            dma((groups, max(rows // 256, 1))),
        ],
        compiler_params=pltpu.CompilerParams(
            collective_id=0, has_side_effects=True, vmem_limit_bytes=60 * 1024 * 1024
        ),
        name="mixers",
    )(tokens, mix_gain, gate_weight, mix_weight, value_weight, out_weight, jnp.transpose(conv_taps, (1, 0, 2)))


def solution(mesh):
    return jax.shard_map(
        shards,
        mesh=mesh,
        in_specs=(
            P(("grp", "sp"), "tp"),
            P(),
            P(None, "sp", "tp"),
            P(None, "sp", "tp"),
            P(None, "sp", "tp"),
            P(None, "sp", "tp"),
            P(None, None, "tp"),
        ),
        out_specs=P(("grp", "sp"), "tp"),
        check_vma=False,
    )
```

time: 157 us -> 130 us (0.83)
  the two profiles are of different devices: /device:TPU:25 before, /device:TPU:0 now
where the time goes in v2:
time: 130 us
  Pallas kernels  128 us (98%)
  local copies, waits for them, and re-layouts  1.87 us (1%)
    pallas_call x1, Pallas kernels, shards(): pl.pallas_call(functools.partial(kernel, (groups, n, tps, lows, gathers,...  128 us

profile of v2, /device:TPU:0, one launch (start us, length us, event | category | flops | bytes accessed | tf_op | source)
XLA Modules:
  0.0 129.7 jit_solution(101876248311510668)
XLA Ops:
  0.0 127.8 %mixers.1 = bf16[512,512]{1,0:T(8,128)(2,1)} custom-call(bf16[512,512]{1,0:T(8,128)(2,1)} %tokens.1, bf16[2,2048]{1,0:T(2,128)(2,1)} %gain.1, bf16[2,512,512]{2,1,0:T(8,128)(2,1)} %gate_w.1, bf16[2,512,512]{2,1,0:T(8,128)(2,1)} %mix_w.1, bf16[2,512,512]{2,1,0:T(8,128)(2,1)} %value_w.1, bf16[2,512,512]{2,1,0:T(8,128)(2,1)} %out_w.1, bf16[3,2,512]{2,1,0:T(2,128)(2,1)} %bitcast.1), custom_call_target="tpu_custom_call" | custom-call | tf_op jit(solution)/shard_map/mixers/pallas_call | solution.py:813
  127.8 1.9 %copy.9 = bf16[512,512]{1,0:T(8,128)(2,1)} copy(bf16[512,512]{1,0:T(8,128)(2,1)} %mixers.1) | data formatting | bytes 1048576

commit v3 on v2

--- a/solution.py
+++ b/solution.py
@@ -351,16 +351,22 @@
                 stream = (resid[g, at : at + count, :].astype(jnp.float32) + product).astype(jnp.bfloat16)
                 resid[g, at : at + count, :] = stream
                 acts[1, g * size + at : g * size + at + count, own] = stream
+            if eager and g > 0:
+                with scope(f"sturn{g - 1}"):
+                    coming[g - 1][3]()
             coming[g][0]()
         for g in parts:
             hook("stream_turn", g)
             with scope(f"sturn{g}"):
-                coming[g][1]()
+                if not eager or g == groups - 1:
+                    coming[g][3]()
+                coming[g][4]()
 
         going = {(cut, g): deep_gather(cut, g, sends) for cut in range(cuts) for g in parts}
 
-        def fill(cut, g):
-            deep[g, :, cut_columns(my_grp, my_tp, cut)] = convolve(layers - 1, g, HALO, rows, cut * half, half)
+        def fill(cut, g, low=0, length=rows):
+            deep[g, low : low + length, cut_columns(my_grp, my_tp, cut)] = convolve(
+                layers - 1, g, HALO + low, length, cut * half, half)
 
         for g in parts:
             hook("stream_finish", g)
@@ -386,12 +392,15 @@
             with scope("vneed"):
                 need(line_of(final_first + 2))
             with scope("second"):
-                for g in parts:
-                    for at, count in spans:
+                assert len(spans) == groups
+                for u, (at, count) in enumerate(spans):
+                    for g in parts:
                         project_second(normed[g, at : at + count, :], g, at, count)
-                    fill(1, g)
-        for u in parts:
-            going[cuts - 1, u][0]()
+                        fill(1, g, u * block, block)
+                    going[1, u][0]()
+        else:
+            for u in parts:
+                going[0, u][0]()
         for g in parts:
             hook("second_turn", g)
             with scope(f"turn2_{g}"):
@@ -658,8 +667,6 @@
         def _():
             with scope("gfinish"):
                 g_finish()
-            with scope("gprepare"):
-                prepare(guest_slot)
 
         for m in assisted[2 * len(assisted) // 3 :]:
             event_in(m)
@@ -681,6 +688,12 @@
 
         for g in parts:
             for i, (at, length) in enumerate(guest_spans):
+                @when(helper)
+                def _():
+                    x = tokens_all[guest_slot, g * rows + i * chunk : g * rows + (i + 1) * chunk, :]
+                    there = pl.multiple_of(HALO + guest_slot * rows + i * chunk, HALO)
+                    normed[g, pl.ds(there, chunk), :] = normalize(x, 0)
+
                 with scope(f"guests{g}"):
                     @pl.when(me == 1)
                     def _():
@@ -688,8 +701,9 @@
 
                     @pl.when(me == n - 2)
                     def _():
-                        before = firsts[-1:] if i == 0 else []
-                        run(g, before + seconds[i : i + 1], rows + at, rows + at + length)
+                        begin, amount = seconds[i]
+                        extra = 2 * HALO if i == 0 else 0
+                        run(g, [(begin - extra, amount + extra)], rows + at, rows + at + length)
 
                 @when(helper)
                 def _():
@@ -705,7 +719,7 @@
 
                 @pl.when(me == n - 2)
                 def _():
-                    run(g, firsts[:-1], 0, rows)
+                    run(g, firsts, 0, rows)
 
                 if n > 4:
                     @pl.when(jnp.logical_not(helper))
@@ -728,7 +742,7 @@
                  ("stream_finish", 0, [("i", p[6], 1)]),
                  ("stream_finish", 1, [("i", p[6], 2)]),
                  ("second", 0, [("i", p[7], 1)]),
-                 ("first_turn", 1, [("i", p[7], 2)])]
+                 ("second_turn", 0, [("i", p[7], 2)])]
         assert total == 8
         points = {}
         tasks = []

time: 130 us -> 129 us (level)
  no operation moved by 1% of the time
where the time goes in v3:
time: 129 us
  Pallas kernels  127 us (98%)
  local copies, waits for them, and re-layouts  1.87 us (1%)
    pallas_call x1, Pallas kernels, shards(): pl.pallas_call(functools.partial(kernel, (groups, n, tps, lows, gathers,...  127 us

profile of v3, /device:TPU:0, one launch (start us, length us, event | category | flops | bytes accessed | tf_op | source)
XLA Modules:
  0.0 129.1 jit_solution(3772180173755429611)
XLA Ops:
  0.0 127.2 %mixers.1 = bf16[512,512]{1,0:T(8,128)(2,1)} custom-call(bf16[512,512]{1,0:T(8,128)(2,1)} %tokens.1, bf16[2,2048]{1,0:T(2,128)(2,1)} %gain.1, bf16[2,512,512]{2,1,0:T(8,128)(2,1)} %gate_w.1, bf16[2,512,512]{2,1,0:T(8,128)(2,1)} %mix_w.1, bf16[2,512,512]{2,1,0:T(8,128)(2,1)} %value_w.1, bf16[2,512,512]{2,1,0:T(8,128)(2,1)} %out_w.1, bf16[3,2,512]{2,1,0:T(2,128)(2,1)} %bitcast.1), custom_call_target="tpu_custom_call" | custom-call | tf_op jit(solution)/shard_map/mixers/pallas_call | solution.py:827
  127.2 1.9 %copy.9 = bf16[512,512]{1,0:T(8,128)(2,1)} copy(bf16[512,512]{1,0:T(8,128)(2,1)} %mixers.1) | data formatting | bytes 1048576
